TPU v7x, 256 devices: a whole 4x4x8 slice. The times are simulated.
256 devices in a mesh: rep: 2 (over z_hi), fs: 16 (over z_lo, x), tp: 8 (over y, core).
Axes of the slice: x: 4, y: 4, z: 8 (z_hi: 2, z_lo: 4; z = z_hi * 4 + z_lo), core: 2. Of those that a mesh axis runs over, the one named last changes fastest.
Arguments:
- tokens: bfloat16 [32768, 2048], P(('rep', 'fs'), 'tp'), may hold values from -6 to 6
- mix_in_gain: bfloat16 [2048], replicated, may hold values from 0.099609375 to 1.8984375
- bgate_weight: bfloat16 [2048, 2048], P('fs', 'tp'), may hold values from -0.125 to 0.125
- cgate_weight: bfloat16 [2048, 2048], P('fs', 'tp'), may hold values from -0.125 to 0.125
- value_weight: bfloat16 [2048, 2048], P('fs', 'tp'), may hold values from -0.125 to 0.125
- conv_taps: bfloat16 [3, 2048], replicated, may hold values from -3 to 3
- out_weight: bfloat16 [2048, 2048], P('tp', 'fs'), may hold values from -0.41984465 to 0.41984465
- mix_out_gain: bfloat16 [2048], replicated, may hold values from 0.099609375 to 1.8984375
- ffn_in_gain: bfloat16 [2048], replicated, may hold values from 0.099609375 to 1.8984375
- up_weight: bfloat16 [2048, 8192], P('fs', 'tp'), may hold values from -0.125 to 0.125
- down_weight: bfloat16 [8192, 2048], P('tp', 'fs'), may hold values from -0.20992233 to 0.20992233
- ffn_out_gain: bfloat16 [2048], replicated, may hold values from 0.099609375 to 1.8984375
Outputs:
- result: bfloat16 [32768, 2048], P(('rep', 'fs'), 'tp')
All inputs are finite; a program needn't handle non-finite values.
Results may differ from a plain program's by a relative error of at most 0.02.
Values may be sent and summed in bfloat16 or wider, within the bound.
A program may use at most 128 MiB of HBM per device.

v0:
```python
import jax
import jax.numpy as jnp
from jax import lax
from jax.sharding import Mesh
from jax.sharding import PartitionSpec as P

LEN = 256
FS = ("fs_0", "fs_1")
REP_FS = ("rep", "fs_0", "fs_1")
epsilon = 1e-06


def in_order(pieces, dim):
    pieces = jnp.moveaxis(pieces, 0, dim)
    shape = pieces.shape
    return pieces.reshape(*shape[:dim], shape[dim] * shape[dim + 1], *shape[dim + 2 :])


def from_everyone(x, axis):
    length = lax.axis_size(axis)
    return lax.all_to_all(jnp.broadcast_to(x[None], (length, *x.shape)), axis, 0, 0, tiled=True)


def gathered_copies(x, axis, dim):
    return in_order(from_everyone(x, axis), dim)


def in_blocks(x, dim, length):
    before, after = (x.shape[:dim], x.shape[dim + 1 :])
    return jnp.moveaxis(x.reshape(*before, length, -1, *after), dim, 0)


def sent_and_summed(x, axis, dim):
    pieces = in_blocks(x, dim, lax.axis_size(axis))
    arrived = lax.all_to_all(pieces, axis, split_axis=0, concat_axis=0, tiled=True)
    return arrived.astype(jnp.float32).sum(axis=0)


def of_everyone(x, axis):
    everything = from_everyone(x, axis)
    return jnp.sum(everything, axis=0)


def all_blocks(x, axes, order):
    pieces = x
    for k in order:
        pieces = lax.all_gather(pieces, axes[k])
    done = order[::-1]
    back = [done.index(k) for k in range(len(axes))]
    pieces = pieces.transpose(*back, *range(len(axes), pieces.ndim))
    return pieces.reshape(-1, *x.shape)


def whole_of(x, axes, order, dim):
    return in_order(all_blocks(x, axes, order), dim)


def normalize(rows, gain):
    rows = rows.astype(jnp.float32)
    factor = lax.rsqrt(jnp.mean(rows * rows, axis=-1, keepdims=True) + epsilon)
    return rows * factor * gain.astype(jnp.float32)


def convolve(inner, taps):
    seqs = inner.reshape(-1, LEN, inner.shape[1])
    padded = jnp.pad(seqs, ((0, 0), (1, 1), (0, 0)))
    weights = taps.astype(jnp.float32)
    out = weights[0] * padded[:, :-2] + weights[1] * padded[:, 1:-1] + weights[2] * padded[:, 2:]
    return out.reshape(inner.shape)


def body(
    tokens,
    mix_in_gain,
    bgate_weight,
    cgate_weight,
    value_weight,
    conv_taps,
    out_weight,
    mix_out_gain,
    ffn_in_gain,
    up_weight,
    down_weight,
    ffn_out_gain,
):
    column = lax.axis_index("tp")
    own_width = tokens.shape[1]
    first = column * own_width
    full_width = mix_in_gain.shape[0]
    whole = lax.all_gather(tokens, "tp", axis=1, tiled=True)
    normed = normalize(whole, mix_in_gain).astype(jnp.bfloat16)

    def add_rows(piece):
        return jnp.dot(normed, piece, preferred_element_type=jnp.float32)

    bgate = add_rows(gathered_copies(bgate_weight, FS, 0))
    cgate = add_rows(gathered_copies(cgate_weight, FS, 0))
    value = add_rows(gathered_copies(value_weight, FS, 0))
    bgate = bgate.astype(jnp.bfloat16)
    cgate = cgate.astype(jnp.bfloat16)
    value = value.astype(jnp.bfloat16)
    channels = bgate.shape[1]
    own_taps = lax.dynamic_slice_in_dim(conv_taps, column * channels, channels, 1)
    inner = cgate.astype(jnp.float32) * value.astype(jnp.float32)
    gated = (bgate.astype(jnp.float32) * convolve(inner, own_taps)).astype(jnp.bfloat16)
    partial_mix = jnp.dot(
        gated, gathered_copies(out_weight, FS, 1), preferred_element_type=jnp.float32
    )
    mixed = sent_and_summed(partial_mix.astype(jnp.bfloat16), "tp", 1)
    power = of_everyone(jnp.sum(mixed * mixed, axis=1), "tp")
    gain_own = lax.dynamic_slice_in_dim(mix_out_gain, first, own_width, 0).astype(jnp.float32)
    scaled = mixed * lax.rsqrt(power[:, None] / full_width + epsilon) * gain_own
    resid_own = (tokens.astype(jnp.float32) + scaled).astype(jnp.bfloat16)
    resid = lax.all_gather(resid_own, "tp", axis=1, tiled=True)
    second = normalize(resid, ffn_in_gain).astype(jnp.bfloat16)
    lifted = jnp.dot(second, whole_of(up_weight, FS, (0, 1), 0), preferred_element_type=jnp.float32)
    active = jnp.square(jnp.maximum(lifted, 0.0)).astype(jnp.bfloat16)
    partial_ffn = jnp.dot(
        active, whole_of(down_weight, FS, (0, 1), 1), preferred_element_type=jnp.float32
    )
    ffn = sent_and_summed(partial_ffn.astype(jnp.bfloat16), "tp", 1)
    ffn_energy = of_everyone(jnp.sum(ffn * ffn, axis=1), "tp")
    out_gain = lax.dynamic_slice_in_dim(ffn_out_gain, first, own_width, 0).astype(jnp.float32)
    closing = ffn * lax.rsqrt(ffn_energy[:, None] / full_width + epsilon) * out_gain
    return (resid_own.astype(jnp.float32) + closing).astype(jnp.bfloat16)


def solution(mesh):
    torus = Mesh(
        mesh.devices.reshape(mesh.shape["rep"], 4, 4, mesh.shape["tp"]),
        ("rep", "fs_0", "fs_1", "tp"),
    )
    return jax.shard_map(
        body,
        mesh=torus,
        in_specs=(
            P(REP_FS, "tp"),
            P(),
            P(FS, "tp"),
            P(FS, "tp"),
            P(FS, "tp"),
            P(),
            P("tp", FS),
            P(),
            P(),
            P(FS, "tp"),
            P("tp", FS),
            P(),
        ),
        out_specs=P(REP_FS, "tp"),
        check_vma=False,
    )
```

profile of v0, /device:TPU:1, one launch (start us, length us, event | category | flops | bytes accessed | tf_op | source)
XLA Modules:
  0.0 391.8 jit_solution(6726258593251835402)
XLA Ops:
  6.5 0.0 all-gather.19.cloned.1.call-start
  6.5 0.7 all-gather.19.cloned.1.call-update
  7.3 0.0 copy-start.5
  7.3 0.0 all-gather.15.cloned.1.call-start
  7.3 0.7 all-gather.15.cloned.1.call-update
  8.0 0.0 all-gather.11.cloned.1.call-start
  8.1 0.7 all-gather.11.cloned.1.call-update
  8.8 0.0 all-gather.21.cloned.1.call-start
  8.8 36.9 %all-gather.19.cloned.1.call-done = bf16[4096,128]{1,0:T(8,128)(2,1)} async-done(((bf16[1024,128]{1,0:T(8,128)(2,1)}), bf16[4096,128]{1,0:T(8,128)(2,1)}) %all-gather.19.cloned.1.call-update) | async-done | bytes 1048592 | tf_op jit(solution)/shard_map/all_gather | solution.py:47
  45.7 0.0 all-gather.21.cloned.1.call-update
  45.8 0.9 broadcast_in_dim.13
  46.7 0.0 copy-start.4
  46.7 40.9 %all_to_all.42 = bf16[16,128,256]{2,1,0:T(8,128)(2,1)S(1)} all-to-all(bf16[16,128,256]{2,1,0:T(8,128)(2,1)S(1)} %broadcast_in_dim.13), channel_id=1, replica_groups=mesh['rep'=2,'fs_0'=4,'fs_1'=4,'tp'=8] {'fs_0','fs_1'}, dimensions={0} | all-to-all | bytes 2097152 | tf_op jit(solution)/shard_map/all_to_all | solution.py:21
  87.6 0.0 copy-done.3
  87.6 1.1 broadcast_in_dim.14
  88.7 9.8 %all-to-all-start.2 = ((bf16[16,128,256]{2,1,0:T(8,128)(2,1)}), bf16[16,128,256]{2,1,0:T(8,128)(2,1)S(1)}, u32[]{:S(2)}, u32[]{:S(2)}) async-start(bf16[16,128,256]{2,1,0:T(8,128)(2,1)} %broadcast_in_dim.14), calls=%async_computation.2 | async-start | bytes 2097152 | tf_op jit(solution)/shard_map/all_to_all | solution.py:21
  98.5 0.1 copy.31
  98.6 21.9 %all-to-all-done.2 = bf16[16,128,256]{2,1,0:T(8,128)(2,1)S(1)} async-done(((bf16[16,128,256]{2,1,0:T(8,128)(2,1)}), bf16[16,128,256]{2,1,0:T(8,128)(2,1)S(1)}, u32[]{:S(2)}, u32[]{:S(2)}) %all-to-all-start.2) | async-done | bytes 1048608 | tf_op jit(solution)/shard_map/all_to_all | solution.py:21
  120.5 1.1 broadcast_in_dim.15
  121.5 7.9 %all-to-all-start.3 = ((bf16[16,256,128]{1,2,0:T(8,128)(2,1)}), bf16[16,256,128]{1,2,0:T(8,128)(2,1)S(1)}, u32[]{:S(2)}, u32[]{:S(2)}) async-start(bf16[16,256,128]{1,2,0:T(8,128)(2,1)} %broadcast_in_dim.15), calls=%async_computation.3 | async-start | bytes 2097152 | tf_op jit(solution)/shard_map/all_to_all | solution.py:21
  129.4 0.7 dynamic-slice_convert_fusion
  130.1 21.5 %all-to-all-done.3 = bf16[16,256,128]{1,2,0:T(8,128)(2,1)S(1)} async-done(((bf16[16,256,128]{1,2,0:T(8,128)(2,1)}), bf16[16,256,128]{1,2,0:T(8,128)(2,1)S(1)}, u32[]{:S(2)}, u32[]{:S(2)}) %all-to-all-start.3) | async-done | bytes 1048608 | tf_op jit(solution)/shard_map/all_to_all | solution.py:21
  151.6 0.0 copy-done.4
  151.6 1.2 broadcast_in_dim.12
  152.8 7.8 %all-to-all-start = ((bf16[16,128,256]{2,1,0:T(8,128)(2,1)}), bf16[16,128,256]{2,1,0:T(8,128)(2,1)}, u32[]{:S(2)}, u32[]{:S(2)}) async-start(bf16[16,128,256]{2,1,0:T(8,128)(2,1)} %broadcast_in_dim.12), calls=%async_computation | async-start | bytes 2097152 | tf_op jit(solution)/shard_map/all_to_all | solution.py:21
  160.6 0.0 all-gather.17.cloned.1.call-start
  160.7 0.0 copy-done.6
  160.7 0.0 all-gather.15.cloned.1.call-done
  160.7 0.5 all-gather.17.cloned.1.call-update
  161.2 0.0 all-gather.11.cloned.1.call-done
  161.2 3.2 fusion
  164.5 0.3 copy-done.1
  164.7 1.3 fusion.13
  166.0 1.3 fusion.12
  167.4 0.3 multiply_add_fusion
  167.7 15.1 %all-to-all-done = bf16[16,128,256]{2,1,0:T(8,128)(2,1)} async-done(((bf16[16,128,256]{2,1,0:T(8,128)(2,1)}), bf16[16,128,256]{2,1,0:T(8,128)(2,1)}, u32[]{:S(2)}, u32[]{:S(2)}) %all-to-all-start) | async-done | bytes 1048608 | tf_op jit(solution)/shard_map/all_to_all | solution.py:21
  182.8 8.8 %convolution_convert_fusion = bf16[1024,2048]{1,0:T(8,128)(2,1)} fusion(bf16[256,2048]{0,1:T(8,128)(2,1)S(1)} %bitcast.55, f32[1024,256]{1,0:T(8,128)S(1)} %bitcast.58, bf16[2048,256]{1,0:T(8,128)(2,1)} %bitcast, bf16[1024,2048]{1,0:T(8,128)(2,1)} %all-gather.11.cloned.1.call-done, f32[2048]{0:T(1024)S(1)} %convert_element_type.79, ...), kind=kOutput, calls=%fused_computation.18 | convolution fusion | flops 2159017984 | bytes 11546624 | tf_op jit(solution)/shard_map/dot_general | solution.py:106
  191.7 2.5 copy.46
  194.1 56.0 %all_to_all.43 = bf16[8,1024,256]{2,1,0:T(8,128)(2,1)S(1)} all-to-all(bf16[8,1024,256]{2,1,0:T(8,128)(2,1)S(1)} %bitcast.44), channel_id=1, replica_groups=mesh['rep'=2,'fs_0'=4,'fs_1'=4,'tp'=8] {'tp'}, dimensions={0} | all-to-all | bytes 8388608 | tf_op jit(solution)/shard_map/all_to_all | solution.py:35
  250.2 0.6 convert_reduce_fusion.1
  250.8 0.2 multiply_reduce_fusion.1
  251.0 0.6 broadcast_in_dim.16
  251.6 4.2 %all-to-all-start.5 = ((f32[8,1,1024]{2,1,0:T(1,128)}), f32[8,1,1024]{2,1,0:T(1,128)S(1)}, u32[]{:S(2)}, u32[]{:S(2)}) async-start(f32[8,1,1024]{2,1,0:T(1,128)} %broadcast_in_dim.16), calls=%async_computation.5 | async-start | bytes 65536 | tf_op jit(solution)/shard_map/all_to_all | solution.py:21
  255.8 0.0 all-gather.13.cloned.1.call-start
  255.8 0.8 dynamic-slice_convert_fusion.2
  256.6 4.0 %all-to-all-done.5 = f32[8,1,1024]{2,1,0:T(1,128)S(1)} async-done(((f32[8,1,1024]{2,1,0:T(1,128)}), f32[8,1,1024]{2,1,0:T(1,128)S(1)}, u32[]{:S(2)}, u32[]{:S(2)}) %all-to-all-start.5) | async-done | bytes 32800 | tf_op jit(solution)/shard_map/all_to_all | solution.py:21
  260.6 1.1 add_convert_fusion.1
  261.7 0.0 all-gather.13.cloned.1.call-update
  261.7 0.0 all-gather.21.cloned.1.call-done
  261.8 4.5 %copy.35 = bf16[4,4,1024,128]{3,2,1,0:T(8,128)(2,1)} copy(bf16[4,4,1024,128]{3,2,0,1:T(8,128)(2,1)} %bitcast.47) | data formatting | bytes 8388608 | tf_op jit(solution)/shard_map/transpose | solution.py:50
  266.3 6.4 %copy.36 = bf16[1024,16,128]{0,2,1:T(8,128)(2,1)} copy(bf16[1024,16,128]{2,0,1:T(8,128)(2,1)} %bitcast.45) | data formatting | bytes 8388608 | tf_op jit(solution)/shard_map/transpose | solution.py:14
  272.7 5.0 %copy.34 = bf16[4,4,128,1024]{3,2,1,0:T(8,128)(2,1)} copy(bf16[4,4,128,1024]{3,2,0,1:T(8,128)(2,1)} %bitcast.48) | data formatting | bytes 8388608 | tf_op jit(solution)/shard_map/transpose | solution.py:50
  277.7 22.9 %all-gather.13.cloned.1.call-done = bf16[1024,2048]{1,0:T(8,128)(2,1)} async-done(((bf16[1024,256]{1,0:T(8,128)(2,1)}), bf16[1024,2048]{1,0:T(8,128)(2,1)}) %all-gather.13.cloned.1.call-update) | async-done | bytes 4194320 | tf_op jit(solution)/shard_map/all_gather | solution.py:114
  300.6 3.1 fusion.3
  303.7 14.6 %convolution_convert_fusion.1 = bf16[1024,2048]{1,0:T(8,128)(2,1)} fusion(bf16[1024,2048]{0,1:T(8,128)(2,1)} %bitcast.49, bf16[2048,1024]{1,0:T(8,128)(2,1)} %bitcast.50, bf16[1024,2048]{1,0:T(8,128)(2,1)} %all-gather.13.cloned.1.call-done, f32[2048]{0:T(1024)S(1)} %convert_element_type.95, f32[1024]{0:T(1024)S(1)} %add_rsqrt_fusion.1), kind=kOutput, calls=%fused_computation.19 | convolution fusion | flops 8603566080 | bytes 16789504 | tf_op jit(solution)/shard_map/dot_general | solution.py:118
  318.3 2.5 copy.45
  320.8 52.6 %all_to_all.44 = bf16[8,1024,256]{2,1,0:T(8,128)(2,1)S(1)} all-to-all(bf16[8,1024,256]{2,1,0:T(8,128)(2,1)S(1)} %bitcast.46), channel_id=1, replica_groups=mesh['rep'=2,'fs_0'=4,'fs_1'=4,'tp'=8] {'tp'}, dimensions={0} | all-to-all | bytes 8388608 | tf_op jit(solution)/shard_map/all_to_all | solution.py:35
  373.4 0.6 convert_reduce_fusion
  374.0 0.2 multiply_reduce_fusion
  374.2 0.6 broadcast_in_dim.17
  374.8 4.3 %all-to-all-start.7 = ((f32[8,1,1024]{2,1,0:T(1,128)}), f32[8,1,1024]{2,1,0:T(1,128)S(1)}, u32[]{:S(2)}, u32[]{:S(2)}) async-start(f32[8,1,1024]{2,1,0:T(1,128)} %broadcast_in_dim.17), calls=%async_computation.7 | async-start | bytes 65536 | tf_op jit(solution)/shard_map/all_to_all | solution.py:21
  379.1 0.8 dynamic-slice_convert_fusion.1
  379.9 4.0 %all-to-all-done.7 = f32[8,1,1024]{2,1,0:T(1,128)S(1)} async-done(((f32[8,1,1024]{2,1,0:T(1,128)}), f32[8,1,1024]{2,1,0:T(1,128)S(1)}, u32[]{:S(2)}, u32[]{:S(2)}) %all-to-all-start.7) | async-done | bytes 32800 | tf_op jit(solution)/shard_map/all_to_all | solution.py:21
  383.9 1.1 add_convert_fusion
  (20 shorter events, 0.1 us)
Async XLA Ops:
  6.5 81.1 %copy-start.3 = (bf16[128,256]{1,0:T(8,128)(2,1)S(1)}, bf16[128,256]{1,0:T(8,128)(2,1)}, u32[]{:S(2)}) copy-start(bf16[128,256]{1,0:T(8,128)(2,1)} %param.16) | copy-start | bytes 196612
  6.5 39.2 %all-gather.19.cloned.1.call-start = ((), (), s32[]{:S(2)}) async-start(), calls=%async_computation.12 | async-start | bytes 1310720 | tf_op jit(solution)/shard_map/all_gather | solution.py:47
  7.3 91.2 %copy-start.5 = (bf16[256,128]{1,0:T(8,128)(2,1)S(1)}, bf16[256,128]{1,0:T(8,128)(2,1)}, u32[]{:S(2)}) copy-start(bf16[256,128]{1,0:T(8,128)(2,1)} %param.18) | copy-start | bytes 196612
  7.3 153.4 %all-gather.15.cloned.1.call-start = ((), (), s32[]{:S(2)}) async-start(), calls=%async_computation.10 | async-start | bytes 1310720 | tf_op jit(solution)/shard_map/all_gather | solution.py:47
  8.0 153.2 %all-gather.11.cloned.1.call-start = ((), (), s32[]{:S(2)}) async-start(), calls=%async_computation.8 | async-start | bytes 4718592 | tf_op jit(solution)/shard_map/all_gather | solution.py:90
  8.8 253.0 %all-gather.21.cloned.1.call-start = ((), (), s32[]{:S(2)}) async-start(), calls=%async_computation.13 | async-start | bytes 5242880 | tf_op jit(solution)/shard_map/all_gather | solution.py:47
  46.7 104.9 %copy-start.4 = (bf16[128,256]{1,0:T(8,128)(2,1)S(1)}, bf16[128,256]{1,0:T(8,128)(2,1)}, u32[]{:S(2)}) copy-start(bf16[128,256]{1,0:T(8,128)(2,1)} %param.14) | copy-start | bytes 196612
  88.7 72.0 %copy-start.6 = (bf16[2048]{0:T(1024)(128)(2,1)S(1)}, bf16[2048]{0:T(1024)(128)(2,1)}, u32[]{:S(2)}) copy-start(bf16[2048]{0:T(1024)(128)(2,1)} %param.13) | copy-start | bytes 12292
  88.7 31.8 %all-to-all-start.2 = ((bf16[16,128,256]{2,1,0:T(8,128)(2,1)}), bf16[16,128,256]{2,1,0:T(8,128)(2,1)S(1)}, u32[]{:S(2)}, u32[]{:S(2)}) async-start(bf16[16,128,256]{2,1,0:T(8,128)(2,1)} %broadcast_in_dim.14), calls=%async_computation.2 | async-start | bytes 2097152 | tf_op jit(solution)/shard_map/all_to_all | solution.py:21
  121.5 30.1 %all-to-all-start.3 = ((bf16[16,256,128]{1,2,0:T(8,128)(2,1)}), bf16[16,256,128]{1,2,0:T(8,128)(2,1)S(1)}, u32[]{:S(2)}, u32[]{:S(2)}) async-start(bf16[16,256,128]{1,2,0:T(8,128)(2,1)} %broadcast_in_dim.15), calls=%async_computation.3 | async-start | bytes 2097152 | tf_op jit(solution)/shard_map/all_to_all | solution.py:21
  152.8 30.1 %all-to-all-start = ((bf16[16,128,256]{2,1,0:T(8,128)(2,1)}), bf16[16,128,256]{2,1,0:T(8,128)(2,1)}, u32[]{:S(2)}, u32[]{:S(2)}) async-start(bf16[16,128,256]{2,1,0:T(8,128)(2,1)} %broadcast_in_dim.12), calls=%async_computation | async-start | bytes 2097152 | tf_op jit(solution)/shard_map/all_to_all | solution.py:21
  160.6 112.1 %all-gather.17.cloned.1.call-start = ((), (), s32[]{:S(2)}) async-start(), calls=%async_computation.11 | async-start | bytes 5242880 | tf_op jit(solution)/shard_map/all_gather | solution.py:47
  161.2 3.5 copy-start.1
  250.2 10.5 %copy-start.2 = (bf16[1024,256]{1,0:T(8,128)(2,1)S(1)}, bf16[1024,256]{1,0:T(8,128)(2,1)}, u32[]{:S(2)}) copy-start(bf16[1024,256]{1,0:T(8,128)(2,1)} %param.12) | copy-start | bytes 1572868
  250.2 11.5 %copy-start.7 = (bf16[2048]{0:T(1024)(128)(2,1)S(1)}, bf16[2048]{0:T(1024)(128)(2,1)}, u32[]{:S(2)}) copy-start(bf16[2048]{0:T(1024)(128)(2,1)} %param.20) | copy-start | bytes 12292
  251.6 9.0 %all-to-all-start.5 = ((f32[8,1,1024]{2,1,0:T(1,128)}), f32[8,1,1024]{2,1,0:T(1,128)S(1)}, u32[]{:S(2)}, u32[]{:S(2)}) async-start(f32[8,1,1024]{2,1,0:T(1,128)} %broadcast_in_dim.16), calls=%async_computation.5 | async-start | bytes 65536 | tf_op jit(solution)/shard_map/all_to_all | solution.py:21
  255.8 44.7 %all-gather.13.cloned.1.call-start = ((), (), s32[]{:S(2)}) async-start(), calls=%async_computation.9 | async-start | bytes 4718592 | tf_op jit(solution)/shard_map/all_gather | solution.py:114
  373.4 10.5 %copy-start = (bf16[1024,256]{1,0:T(8,128)(2,1)S(1)}, bf16[1024,256]{1,0:T(8,128)(2,1)}, u32[]{:S(2)}) copy-start(bf16[1024,256]{1,0:T(8,128)(2,1)} %add_convert_fusion.1) | copy-start | bytes 1572868
  374.8 9.0 %all-to-all-start.7 = ((f32[8,1,1024]{2,1,0:T(1,128)}), f32[8,1,1024]{2,1,0:T(1,128)S(1)}, u32[]{:S(2)}, u32[]{:S(2)}) async-start(f32[8,1,1024]{2,1,0:T(1,128)} %broadcast_in_dim.17), calls=%async_computation.7 | async-start | bytes 65536 | tf_op jit(solution)/shard_map/all_to_all | solution.py:21
Sparse Core Ops, SparseCore 0:
  9.1 36.5 all-gather.18
  47.5 43.0 all-gather.14
  92.5 42.0 all-gather.10
  136.3 62.9 all-gather.20
  200.9 51.1 all-gather.16
  261.8 38.7 all-gather.12
where the time goes:
time: 393 us; the launch traced here: 392 us
  blocking collectives  150 us (38%)
  waiting for transfers between devices  129 us (33%)
  starting transfers between devices  34.2 us (9%)
  local copies, waits for them, and re-layouts  26.7 us (7%)
  matrix products  26.1 us (7%)
  between operations  13.7 us (3%)
  other arithmetic  12.6 us (3%)
    all_to_all x2, blocking collectives, sent_and_summed(): lax.all_to_all(pieces, axis, split_axis=0, concat_axis=0, tiled=True)  109 us
    all_to_all x5, waiting for transfers between devices, from_everyone(): lax.all_to_all(jnp.broadcast_to(x[None], (length, *x.shape)), axis, 0, 0,...  66.4 us
    all_to_all x1, blocking collectives, from_everyone(): lax.all_to_all(jnp.broadcast_to(x[None], (length, *x.shape)), axis, 0, 0,...  40.9 us
    all_gather x4, waiting for transfers between devices, all_blocks(): pieces = lax.all_gather(pieces, axes[k])  37 us
    all_to_all x5, starting transfers between devices, from_everyone(): lax.all_to_all(jnp.broadcast_to(x[None], (length, *x.shape)), axis, 0, 0,...  34 us
    all_gather x1, waiting for transfers between devices, body(): resid = lax.all_gather(resid_own, 'tp', axis=1, tiled=True)  22.9 us
    dot_general x1, matrix products, body(): jnp.dot(active, whole_of(down_weight, FS, (0, 1), 1), preferred_element_t...  14.6 us
    transpose x2, local copies, waits for them, and re-layouts, all_blocks(): pieces = pieces.transpose(*back, *range(len(axes), pieces.ndim))  9.5 us
  transfers between devices with their start and end apart: 11, of which 7 were waited for; matrix products, arithmetic and copies ran while one was open for 11% of the time, Pallas kernels for 0%

commit v1 on v0

--- a/solution.py
+++ b/solution.py
@@ -8,6 +8,27 @@
 FS = ("fs_0", "fs_1")
 REP_FS = ("rep", "fs_0", "fs_1")
 epsilon = 1e-06
+
+
+def collect(x, axis, dim):
+    devices, position, rows = (lax.axis_size(axis), lax.axis_index(axis), x.shape[dim])
+    forward = [(i, (i + 1) % devices) for i in range(devices)]
+    left = [(i, (i - 1) % devices) for i in range(devices)]
+    result = jnp.zeros((*x.shape[:dim], devices * rows, *x.shape[dim + 1 :]), x.dtype)
+    result = lax.dynamic_update_slice_in_dim(result, x, position * rows, axis=dim)
+    from_left = from_right = x
+    halfway = devices // 2
+    for step in range(1, halfway + 1):
+        from_left = lax.ppermute(from_left, axis, forward)
+        result = lax.dynamic_update_slice_in_dim(
+            result, from_left, (position - step) % devices * rows, axis=dim
+        )
+        if step < devices - halfway:
+            from_right = lax.ppermute(from_right, axis, left)
+            result = lax.dynamic_update_slice_in_dim(
+                result, from_right, (position + step) % devices * rows, axis=dim
+            )
+    return result
 
 
 def in_order(pieces, dim):
@@ -111,7 +132,7 @@
     gain_own = lax.dynamic_slice_in_dim(mix_out_gain, first, own_width, 0).astype(jnp.float32)
     scaled = mixed * lax.rsqrt(power[:, None] / full_width + epsilon) * gain_own
     resid_own = (tokens.astype(jnp.float32) + scaled).astype(jnp.bfloat16)
-    resid = lax.all_gather(resid_own, "tp", axis=1, tiled=True)
+    resid = collect(resid_own, "tp", 1)
     second = normalize(resid, ffn_in_gain).astype(jnp.bfloat16)
     lifted = jnp.dot(second, whole_of(up_weight, FS, (0, 1), 0), preferred_element_type=jnp.float32)
     active = jnp.square(jnp.maximum(lifted, 0.0)).astype(jnp.bfloat16)

time: 393 us -> 406 us (1.033)
  waiting for transfers between devices: 129 us -> 119 us
  starting transfers between devices: 34.2 us -> 43.1 us
  local copies, waits for them, and re-layouts: 26.7 us -> 35.4 us
    all_gather x1 -> x0, waiting for transfers between devices: 22.9 us -> none  [body(): resid = lax.all_gather(resid_own, 'tp', axis=1, tiled=True)]
    ppermute x0 -> x7, waiting for transfers between devices: none -> 13.4 us  [the longest x4 11.2 us: collect(): from_left = lax.ppermute(from_left, axis, forward)]
    ppermute x0 -> x7, starting transfers between devices: none -> 8.96 us  [the longest x4 5.94 us: collect(): from_left = lax.ppermute(from_left, axis, forward)]
    dynamic_update_slice x0 -> x7, local copies, waits for them, and re-layouts: none -> 6.2 us  [the longest x4 3.49 us: collect(): lax.dynamic_update_slice_in_dim(result, from_left, (position - step) % de...]
    all_to_all x2, blocking collectives: 109 us -> 114 us  [sent_and_summed(): lax.all_to_all(pieces, axis, split_axis=0, concat_axis=0, tiled=True)]
  transfers between devices with their start and end apart: 11 -> 17, of which waited for: 7 -> 10; matrix products, arithmetic and copies ran while one was open for 11% -> 12% of each run, Pallas kernels for 0% -> 0%
where the time goes in v1:
time: 406 us; the launch traced here: 404 us
  blocking collectives  154 us (38%)
  waiting for transfers between devices  119 us (29%)
  starting transfers between devices  43.1 us (11%)
  local copies, waits for them, and re-layouts  35.4 us (9%)
  matrix products  26.1 us (6%)
  between operations  13.4 us (3%)
  other arithmetic  12.6 us (3%)
    all_to_all x2, blocking collectives, sent_and_summed(): lax.all_to_all(pieces, axis, split_axis=0, concat_axis=0, tiled=True)  114 us
    all_to_all x5, waiting for transfers between devices, from_everyone(): lax.all_to_all(jnp.broadcast_to(x[None], (length, *x.shape)), axis, 0, 0,...  66.5 us
    all_to_all x1, blocking collectives, from_everyone(): lax.all_to_all(jnp.broadcast_to(x[None], (length, *x.shape)), axis, 0, 0,...  40.9 us
    all_gather x4, waiting for transfers between devices, all_blocks(): pieces = lax.all_gather(pieces, axes[k])  37 us
    all_to_all x5, starting transfers between devices, from_everyone(): lax.all_to_all(jnp.broadcast_to(x[None], (length, *x.shape)), axis, 0, 0,...  34 us
    dot_general x1, matrix products, body(): jnp.dot(active, whole_of(down_weight, FS, (0, 1), 1), preferred_element_t...  14.6 us
    ppermute x4, waiting for transfers between devices, collect(): from_left = lax.ppermute(from_left, axis, forward)  11.2 us
    transpose x2, local copies, waits for them, and re-layouts, all_blocks(): pieces = pieces.transpose(*back, *range(len(axes), pieces.ndim))  9.34 us
  transfers between devices with their start and end apart: 17, of which 10 were waited for; matrix products, arithmetic and copies ran while one was open for 12% of the time, Pallas kernels for 0%

profile of v1, /device:TPU:1, one launch (start us, length us, event | category | flops | bytes accessed | tf_op | source)
XLA Modules:
  0.0 404.4 jit_solution(9851091496327775370)
XLA Ops:
  6.5 0.7 all-gather.16.cloned.1.call-update
  7.3 0.7 all-gather.12.cloned.1.call-update
  8.1 0.7 all-gather.10.cloned.1.call-update
  8.8 36.9 %all-gather.16.cloned.1.call-done = bf16[4096,128]{1,0:T(8,128)(2,1)} async-done(((bf16[1024,128]{1,0:T(8,128)(2,1)}), bf16[4096,128]{1,0:T(8,128)(2,1)}) %all-gather.16.cloned.1.call-update) | async-done | bytes 1048592 | tf_op jit(solution)/shard_map/all_gather | solution.py:68
  45.8 0.9 broadcast_in_dim.15
  46.7 40.9 %all_to_all.42 = bf16[16,128,256]{2,1,0:T(8,128)(2,1)S(1)} all-to-all(bf16[16,128,256]{2,1,0:T(8,128)(2,1)S(1)} %broadcast_in_dim.15), channel_id=1, replica_groups=mesh['rep'=2,'fs_0'=4,'fs_1'=4,'tp'=8] {'fs_0','fs_1'}, dimensions={0} | all-to-all | bytes 2097152 | tf_op jit(solution)/shard_map/all_to_all | solution.py:42
  87.6 1.2 broadcast_in_dim.16
  88.8 9.8 %all-to-all-start.2 = ((bf16[16,128,256]{2,1,0:T(8,128)(2,1)}), bf16[16,128,256]{2,1,0:T(8,128)(2,1)S(1)}, u32[]{:S(2)}, u32[]{:S(2)}) async-start(bf16[16,128,256]{2,1,0:T(8,128)(2,1)} %broadcast_in_dim.16), calls=%async_computation.2 | async-start | bytes 2097152 | tf_op jit(solution)/shard_map/all_to_all | solution.py:42
  98.6 0.1 copy.31
  98.7 21.9 %all-to-all-done.2 = bf16[16,128,256]{2,1,0:T(8,128)(2,1)S(1)} async-done(((bf16[16,128,256]{2,1,0:T(8,128)(2,1)}), bf16[16,128,256]{2,1,0:T(8,128)(2,1)S(1)}, u32[]{:S(2)}, u32[]{:S(2)}) %all-to-all-start.2) | async-done | bytes 1048608 | tf_op jit(solution)/shard_map/all_to_all | solution.py:42
  120.6 1.2 broadcast_in_dim.17
  121.7 7.9 %all-to-all-start.3 = ((bf16[16,256,128]{1,2,0:T(8,128)(2,1)}), bf16[16,256,128]{1,2,0:T(8,128)(2,1)S(1)}, u32[]{:S(2)}, u32[]{:S(2)}) async-start(bf16[16,256,128]{1,2,0:T(8,128)(2,1)} %broadcast_in_dim.17), calls=%async_computation.3 | async-start | bytes 2097152 | tf_op jit(solution)/shard_map/all_to_all | solution.py:42
  129.6 0.7 fusion.21
  130.3 21.5 %all-to-all-done.3 = bf16[16,256,128]{1,2,0:T(8,128)(2,1)S(1)} async-done(((bf16[16,256,128]{1,2,0:T(8,128)(2,1)}), bf16[16,256,128]{1,2,0:T(8,128)(2,1)S(1)}, u32[]{:S(2)}, u32[]{:S(2)}) %all-to-all-start.3) | async-done | bytes 1048608 | tf_op jit(solution)/shard_map/all_to_all | solution.py:42
  151.8 1.1 broadcast_in_dim.14
  152.9 7.8 %all-to-all-start = ((bf16[16,128,256]{2,1,0:T(8,128)(2,1)}), bf16[16,128,256]{2,1,0:T(8,128)(2,1)}, u32[]{:S(2)}, u32[]{:S(2)}) async-start(bf16[16,128,256]{2,1,0:T(8,128)(2,1)} %broadcast_in_dim.14), calls=%async_computation | async-start | bytes 2097152 | tf_op jit(solution)/shard_map/all_to_all | solution.py:42
  160.9 0.5 all-gather.14.cloned.1.call-update
  161.4 3.2 fusion
  164.6 0.3 copy-done
  164.9 1.3 fusion.13
  166.2 1.3 fusion.12
  167.5 0.3 multiply_add_fusion
  167.8 15.2 %all-to-all-done = bf16[16,128,256]{2,1,0:T(8,128)(2,1)} async-done(((bf16[16,128,256]{2,1,0:T(8,128)(2,1)}), bf16[16,128,256]{2,1,0:T(8,128)(2,1)}, u32[]{:S(2)}, u32[]{:S(2)}) %all-to-all-start) | async-done | bytes 1048608 | tf_op jit(solution)/shard_map/all_to_all | solution.py:42
  183.0 8.8 %convolution_convert_fusion = bf16[1024,2048]{1,0:T(8,128)(2,1)} fusion(bf16[256,2048]{0,1:T(8,128)(2,1)S(1)} %bitcast.55, f32[1024,256]{1,0:T(8,128)S(1)} %bitcast.58, bf16[2048,256]{1,0:T(8,128)(2,1)} %bitcast, bf16[1024,2048]{1,0:T(8,128)(2,1)} %all-gather.10.cloned.1.call-done, f32[2048]{0:T(1024)S(1)} %convert_element_type.79, ...), kind=kOutput, calls=%fused_computation.18 | convolution fusion | flops 2159017984 | bytes 11546624 | tf_op jit(solution)/shard_map/dot_general | solution.py:127
  191.8 2.5 copy.46
  194.3 56.0 %all_to_all.43 = bf16[8,1024,256]{2,1,0:T(8,128)(2,1)S(1)} all-to-all(bf16[8,1024,256]{2,1,0:T(8,128)(2,1)S(1)} %bitcast.44), channel_id=1, replica_groups=mesh['rep'=2,'fs_0'=4,'fs_1'=4,'tp'=8] {'tp'}, dimensions={0} | all-to-all | bytes 8388608 | tf_op jit(solution)/shard_map/all_to_all | solution.py:56
  250.3 0.6 convert_reduce_fusion.1
  250.9 0.2 multiply_reduce_fusion.1
  251.1 0.6 broadcast_in_dim.18
  251.8 4.2 %all-to-all-start.5 = ((f32[8,1,1024]{2,1,0:T(1,128)}), f32[8,1,1024]{2,1,0:T(1,128)S(1)}, u32[]{:S(2)}, u32[]{:S(2)}) async-start(f32[8,1,1024]{2,1,0:T(1,128)} %broadcast_in_dim.18), calls=%async_computation.5 | async-start | bytes 65536 | tf_op jit(solution)/shard_map/all_to_all | solution.py:42
  256.0 0.8 dynamic-slice_convert_fusion.1
  256.8 4.0 all-to-all-done.5
  260.8 2.5 broadcast_in_dim.19
  263.2 1.1 constant_dynamic-update-slice_fusion.7
  264.3 1.0 collective-permute-start
  265.3 6.1 %collective-permute-done = bf16[1024,256]{1,0:T(8,128)(2,1)S(1)} collective-permute-done((bf16[1024,256]{1,0:T(8,128)(2,1)S(1)}, bf16[1024,256]{1,0:T(8,128)(2,1)S(1)}, u32[]{:S(2)}, u32[]{:S(2)}) %collective-permute-start) | collective-permute-done | bytes 524320 | tf_op jit(solution)/shard_map/ppermute | solution.py:22
  271.4 2.5 collective-permute-start.2
  273.9 0.3 collective-permute-done.1
  274.2 0.7 collective-permute-start.3
  274.9 5.1 %collective-permute-done.2 = bf16[1024,256]{1,0:T(8,128)(2,1)S(1)} collective-permute-done((bf16[1024,256]{1,0:T(8,128)(2,1)S(1)}, bf16[1024,256]{1,0:T(8,128)(2,1)S(1)}, u32[]{:S(2)}, u32[]{:S(2)}) %collective-permute-start.2) | collective-permute-done | bytes 524320 | tf_op jit(solution)/shard_map/ppermute | solution.py:22
  280.0 2.5 collective-permute-start.4
  282.5 4.6 %copy.35 = bf16[4,4,1024,128]{3,2,1,0:T(8,128)(2,1)} copy(bf16[4,4,1024,128]{3,2,0,1:T(8,128)(2,1)} %bitcast.47) | data formatting | bytes 8388608 | tf_op jit(solution)/shard_map/transpose | solution.py:71
  287.1 6.4 %copy.36 = bf16[1024,16,128]{0,2,1:T(8,128)(2,1)} copy(bf16[1024,16,128]{2,0,1:T(8,128)(2,1)} %bitcast.45) | data formatting | bytes 8388608 | tf_op jit(solution)/shard_map/transpose | solution.py:35
  293.5 4.8 %copy.34 = bf16[4,4,128,1024]{3,2,1,0:T(8,128)(2,1)} copy(bf16[4,4,128,1024]{3,2,0,1:T(8,128)(2,1)} %bitcast.48) | data formatting | bytes 8388608 | tf_op jit(solution)/shard_map/transpose | solution.py:71
  298.3 2.3 collective-permute-start.5
  300.6 0.9 constant_dynamic-update-slice_fusion.6
  301.5 0.9 constant_dynamic-update-slice_fusion.5
  302.4 0.9 constant_dynamic-update-slice_fusion.4
  303.3 0.9 constant_dynamic-update-slice_fusion.3
  304.2 0.9 constant_dynamic-update-slice_fusion.2
  305.0 1.9 collective-permute-done.5
  306.9 0.9 constant_dynamic-update-slice_fusion.1
  307.8 0.9 constant_dynamic-update-slice_fusion
  308.6 3.1 fusion.3
  311.7 14.6 %convolution_convert_fusion.1 = bf16[1024,2048]{1,0:T(8,128)(2,1)} fusion(bf16[1024,2048]{0,1:T(8,128)(2,1)} %bitcast.49, bf16[2048,1024]{1,0:T(8,128)(2,1)} %bitcast.50, bf16[1024,2048]{1,0:T(8,128)(2,1)} %constant_dynamic-update-slice_fusion, f32[2048]{0:T(1024)S(1)} %convert_element_type.95, f32[1024]{0:T(1024)S(1)} %add_rsqrt_fusion.1), kind=kOutput, calls=%fused_computation.19 | convolution fusion | flops 8603566080 | bytes 16789504 | tf_op jit(solution)/shard_map/dot_general | solution.py:139
  326.4 2.5 copy.45
  328.8 57.5 %all_to_all.44 = bf16[8,1024,256]{2,1,0:T(8,128)(2,1)S(1)} all-to-all(bf16[8,1024,256]{2,1,0:T(8,128)(2,1)S(1)} %bitcast.46), channel_id=1, replica_groups=mesh['rep'=2,'fs_0'=4,'fs_1'=4,'tp'=8] {'tp'}, dimensions={0} | all-to-all | bytes 8388608 | tf_op jit(solution)/shard_map/all_to_all | solution.py:56
  386.4 0.6 convert_reduce_fusion
  386.9 0.2 multiply_reduce_fusion
  387.2 0.6 broadcast_in_dim.20
  387.8 4.3 %all-to-all-start.7 = ((f32[8,1,1024]{2,1,0:T(1,128)}), f32[8,1,1024]{2,1,0:T(1,128)S(1)}, u32[]{:S(2)}, u32[]{:S(2)}) async-start(f32[8,1,1024]{2,1,0:T(1,128)} %broadcast_in_dim.20), calls=%async_computation.7 | async-start | bytes 65536 | tf_op jit(solution)/shard_map/all_to_all | solution.py:42
  392.1 0.8 dynamic-slice_convert_fusion
  392.8 4.0 all-to-all-done.7
  396.9 1.1 add_convert_fusion
  (37 shorter events, 0.4 us)
Async XLA Ops:
  6.5 81.1 %copy-start.2 = (bf16[128,256]{1,0:T(8,128)(2,1)S(1)}, bf16[128,256]{1,0:T(8,128)(2,1)}, u32[]{:S(2)}) copy-start(bf16[128,256]{1,0:T(8,128)(2,1)} %param.16) | copy-start | bytes 196612
  6.5 39.2 %all-gather.16.cloned.1.call-start = ((), (), s32[]{:S(2)}) async-start(), calls=%async_computation.11 | async-start | bytes 1310720 | tf_op jit(solution)/shard_map/all_gather | solution.py:68
  7.3 91.3 %copy-start.4 = (bf16[256,128]{1,0:T(8,128)(2,1)S(1)}, bf16[256,128]{1,0:T(8,128)(2,1)}, u32[]{:S(2)}) copy-start(bf16[256,128]{1,0:T(8,128)(2,1)} %param.18) | copy-start | bytes 196612
  7.3 153.6 %all-gather.12.cloned.1.call-start = ((), (), s32[]{:S(2)}) async-start(), calls=%async_computation.9 | async-start | bytes 1310720 | tf_op jit(solution)/shard_map/all_gather | solution.py:68
  8.0 153.3 %all-gather.10.cloned.1.call-start = ((), (), s32[]{:S(2)}) async-start(), calls=%async_computation.8 | async-start | bytes 4718592 | tf_op jit(solution)/shard_map/all_gather | solution.py:111
  8.8 273.8 %all-gather.18.cloned.1.call-start = ((), (), s32[]{:S(2)}) async-start(), calls=%async_computation.12 | async-start | bytes 5242880 | tf_op jit(solution)/shard_map/all_gather | solution.py:68
  46.7 105.1 %copy-start.3 = (bf16[128,256]{1,0:T(8,128)(2,1)S(1)}, bf16[128,256]{1,0:T(8,128)(2,1)}, u32[]{:S(2)}) copy-start(bf16[128,256]{1,0:T(8,128)(2,1)} %param.14) | copy-start | bytes 196612
  88.8 72.0 %copy-start.5 = (bf16[2048]{0:T(1024)(128)(2,1)S(1)}, bf16[2048]{0:T(1024)(128)(2,1)}, u32[]{:S(2)}) copy-start(bf16[2048]{0:T(1024)(128)(2,1)} %param.13) | copy-start | bytes 12292
  88.8 31.8 %all-to-all-start.2 = ((bf16[16,128,256]{2,1,0:T(8,128)(2,1)}), bf16[16,128,256]{2,1,0:T(8,128)(2,1)S(1)}, u32[]{:S(2)}, u32[]{:S(2)}) async-start(bf16[16,128,256]{2,1,0:T(8,128)(2,1)} %broadcast_in_dim.16), calls=%async_computation.2 | async-start | bytes 2097152 | tf_op jit(solution)/shard_map/all_to_all | solution.py:42
  121.7 30.1 %all-to-all-start.3 = ((bf16[16,256,128]{1,2,0:T(8,128)(2,1)}), bf16[16,256,128]{1,2,0:T(8,128)(2,1)S(1)}, u32[]{:S(2)}, u32[]{:S(2)}) async-start(bf16[16,256,128]{1,2,0:T(8,128)(2,1)} %broadcast_in_dim.17), calls=%async_computation.3 | async-start | bytes 2097152 | tf_op jit(solution)/shard_map/all_to_all | solution.py:42
  152.9 30.1 %all-to-all-start = ((bf16[16,128,256]{2,1,0:T(8,128)(2,1)}), bf16[16,128,256]{2,1,0:T(8,128)(2,1)}, u32[]{:S(2)}, u32[]{:S(2)}) async-start(bf16[16,128,256]{2,1,0:T(8,128)(2,1)} %broadcast_in_dim.14), calls=%async_computation | async-start | bytes 2097152 | tf_op jit(solution)/shard_map/all_to_all | solution.py:42
  160.8 132.7 %all-gather.14.cloned.1.call-start = ((), (), s32[]{:S(2)}) async-start(), calls=%async_computation.10 | async-start | bytes 5242880 | tf_op jit(solution)/shard_map/all_gather | solution.py:68
  161.4 3.5 copy-start
  250.3 12.9 %copy-start.1 = (bf16[1024,256]{1,0:T(8,128)(2,1)S(1)}, bf16[1024,256]{1,0:T(8,128)(2,1)}, u32[]{:S(2)}) copy-start(bf16[1024,256]{1,0:T(8,128)(2,1)} %param.12) | copy-start | bytes 1572868
  250.9 31.6 %copy-start.6 = (bf16[2048]{0:T(1024)(128)(2,1)S(1)}, bf16[2048]{0:T(1024)(128)(2,1)}, u32[]{:S(2)}) copy-start(bf16[2048]{0:T(1024)(128)(2,1)} %param.20) | copy-start | bytes 12292
  251.8 9.0 %all-to-all-start.5 = ((f32[8,1,1024]{2,1,0:T(1,128)}), f32[8,1,1024]{2,1,0:T(1,128)S(1)}, u32[]{:S(2)}, u32[]{:S(2)}) async-start(f32[8,1,1024]{2,1,0:T(1,128)} %broadcast_in_dim.18), calls=%async_computation.5 | async-start | bytes 65536 | tf_op jit(solution)/shard_map/all_to_all | solution.py:42
  264.3 7.1 %collective-permute-start = (bf16[1024,256]{1,0:T(8,128)(2,1)S(1)}, bf16[1024,256]{1,0:T(8,128)(2,1)S(1)}, u32[]{:S(2)}, u32[]{:S(2)}) collective-permute-start(bf16[1024,256]{1,0:T(8,128)(2,1)S(1)} %get-tuple-element.6), channel_id=1, source_target_pairs={{0,1},{1,2},{2,3},{3,4},{4,5},{5,6},{6,7},{7,0},{8,9},{9,10},{10,1... | collective-permute-start | bytes 1572872 | tf_op jit(solution)/shard_map/ppermute | solution.py:22
  265.3 8.9 %collective-permute-start.1 = (bf16[1024,256]{1,0:T(8,128)(2,1)S(1)}, bf16[1024,256]{1,0:T(8,128)(2,1)S(1)}, u32[]{:S(2)}, u32[]{:S(2)}) collective-permute-start(bf16[1024,256]{1,0:T(8,128)(2,1)S(1)} %get-tuple-element.6), channel_id=1, source_target_pairs={{0,7},{1,0},{2,1},{3,2},{4,3},{5,4},{6,5},{7,6},{8,15},{9,8},{10,9... | collective-permute-start | bytes 1572872 | tf_op jit(solution)/shard_map/ppermute | solution.py:27
  271.4 8.6 %collective-permute-start.2 = (bf16[1024,256]{1,0:T(8,128)(2,1)S(1)}, bf16[1024,256]{1,0:T(8,128)(2,1)S(1)}, u32[]{:S(2)}, u32[]{:S(2)}) collective-permute-start(bf16[1024,256]{1,0:T(8,128)(2,1)S(1)} %collective-permute-done), channel_id=1, source_target_pairs={{0,1},{1,2},{2,3},{3,4},{4,5},{5,6},{6,7},{7,0},{8,9},{9,10},{10,1... | collective-permute-start | bytes 1572872 | tf_op jit(solution)/shard_map/ppermute | solution.py:22
  274.2 24.1 %collective-permute-start.3 = (bf16[1024,256]{1,0:T(8,128)(2,1)S(1)}, bf16[1024,256]{1,0:T(8,128)(2,1)S(1)}, u32[]{:S(2)}, u32[]{:S(2)}) collective-permute-start(bf16[1024,256]{1,0:T(8,128)(2,1)S(1)} %collective-permute-done.1), channel_id=1, source_target_pairs={{0,7},{1,0},{2,1},{3,2},{4,3},{5,4},{6,5},{7,6},{8,15},{9,8},{10,9... | collective-permute-start | bytes 1572872 | tf_op jit(solution)/shard_map/ppermute | solution.py:27
  280.0 21.4 %collective-permute-start.4 = (bf16[1024,256]{1,0:T(8,128)(2,1)S(1)}, bf16[1024,256]{1,0:T(8,128)(2,1)S(1)}, u32[]{:S(2)}, u32[]{:S(2)}) collective-permute-start(bf16[1024,256]{1,0:T(8,128)(2,1)S(1)} %collective-permute-done.2), channel_id=1, source_target_pairs={{0,1},{1,2},{2,3},{3,4},{4,5},{5,6},{6,7},{7,0},{8,9},{9,10},{10,1... | collective-permute-start | bytes 1572872 | tf_op jit(solution)/shard_map/ppermute | solution.py:22
  298.3 8.6 %collective-permute-start.5 = (bf16[1024,256]{1,0:T(8,128)(2,1)S(1)}, bf16[1024,256]{1,0:T(8,128)(2,1)S(1)}, u32[]{:S(2)}, u32[]{:S(2)}) collective-permute-start(bf16[1024,256]{1,0:T(8,128)(2,1)S(1)} %collective-permute-done.3), channel_id=1, source_target_pairs={{0,7},{1,0},{2,1},{3,2},{4,3},{5,4},{6,5},{7,6},{8,15},{9,8},{10,9... | collective-permute-start | bytes 1572872 | tf_op jit(solution)/shard_map/ppermute | solution.py:27
  301.5 6.3 %collective-permute-start.6 = (bf16[1024,256]{1,0:T(8,128)(2,1)S(1)}, bf16[1024,256]{1,0:T(8,128)(2,1)S(1)}, u32[]{:S(2)}, u32[]{:S(2)}) collective-permute-start(bf16[1024,256]{1,0:T(8,128)(2,1)S(1)} %collective-permute-done.4), channel_id=1, source_target_pairs={{0,1},{1,2},{2,3},{3,4},{4,5},{5,6},{6,7},{7,0},{8,9},{9,10},{10,1... | collective-permute-start | bytes 1572872 | tf_op jit(solution)/shard_map/ppermute | solution.py:22
  387.8 9.0 %all-to-all-start.7 = ((f32[8,1,1024]{2,1,0:T(1,128)}), f32[8,1,1024]{2,1,0:T(1,128)S(1)}, u32[]{:S(2)}, u32[]{:S(2)}) async-start(f32[8,1,1024]{2,1,0:T(1,128)} %broadcast_in_dim.20), calls=%async_computation.7 | async-start | bytes 65536 | tf_op jit(solution)/shard_map/all_to_all | solution.py:42
Sparse Core Ops, SparseCore 0:
  9.1 36.5 all-gather.15
  47.5 43.0 all-gather.11
  92.5 42.0 all-gather.9
  136.3 63.2 all-gather.17
  201.2 50.9 all-gather.13
